TPU v7x, 32 devices: a whole 2x2x4 slice. The times are simulated.
32 devices in a mesh: grp: 2 (over y), ra: 4 (over z), cb: 4 (over x, core).
Axes of the slice: x: 2, y: 2, z: 4, core: 2. Of those that a mesh axis runs over, the one named last changes fastest.
Arguments:
- tokens: bfloat16 [512, 4096], P('grp', 'cb'), parts along dimension 0, may hold values from -50 to 50
- norm_gains: float32 [3, 4096], P(None, 'cb'), may hold values from 0.1 to 1.9
- gate_weight: float32 [2, 4096, 11264], P(None, 'cb', 'ra'), may hold values from -0.09375 to 0.09375
- value_weight: float32 [2, 4096, 11264], P(None, 'cb', 'ra'), may hold values from -0.09375 to 0.09375
- gate_scale: float32 [2, 11264], P(None, 'ra'), may hold values from 0.3 to 3
- value_scale: float32 [2, 11264], P(None, 'ra'), may hold values from 0.3 to 3
- conv_gate: float32 [2, 3, 11264], P(None, None, 'ra'), may hold values from -3 to 3
- conv_value: float32 [2, 3, 11264], P(None, None, 'ra'), may hold values from -3 to 3
- down_weight: float32 [2, 11264, 4096], P(None, 'ra', 'cb'), may hold values from -0.07537784 to 0.07537784
- down_scale: float32 [2, 4096], P(None, 'cb'), may hold values from 0.3 to 3
Outputs:
- normed_out: bfloat16 [512, 4096], P('grp', 'cb'), parts along dimension 0
There are 2 independent parts, one for each index of `grp`. A program takes and returns all parts, laid end to end along the dimension named above; an argument that names none is the same for every part. Nothing has to cross between parts.
All inputs are finite; a program needn't handle non-finite values.
Results may differ from a plain program's by a relative error of at most 0.012.
The roundings to bfloat16 on the way count: a program that leaves them out, or rounds other values in their place, can miss the bound.
Values may be sent and summed in bfloat16 or wider, within the bound.
A program may use at most 192 MiB of HBM per device.

v0:
```python
import jax
import jax.numpy as jnp
from jax import lax
from jax.sharding import PartitionSpec as P

epsilon = 1e-06
residual_weight = 0.5


def causal_taps(projected, tap_weights):
    tap_count = tap_weights.shape[0]
    row_count = projected.shape[0]
    padded = jnp.pad(projected, ((tap_count - 1, 0), (0, 0)))
    result = jnp.zeros_like(projected)
    for tap_idx in range(tap_count):
        result = result + padded[tap_idx : tap_idx + row_count] * tap_weights[tap_idx]
    return result


def row_inverse(state_wide, model_width):
    squares = lax.psum(jnp.sum(state_wide * state_wide, axis=1, keepdims=True), "cb")
    return lax.rsqrt(squares / model_width + epsilon)


def on_device(
    tokens,
    norm_gains,
    gate_weight,
    value_weight,
    gate_scale,
    value_scale,
    conv_gate,
    conv_value,
    down_weight,
    down_scale,
):
    model_width = lax.axis_size("cb") * tokens.shape[1]
    layer_count = gate_weight.shape[0]
    current = tokens
    for layer_idx in range(layer_count):
        state_wide = current.astype(jnp.float32)
        inverse = row_inverse(state_wide, model_width)
        scaled = (state_wide * norm_gains[layer_idx]).astype(jnp.bfloat16)
        gate_part = jnp.dot(
            scaled, gate_weight[layer_idx].astype(jnp.bfloat16), preferred_element_type=jnp.float32
        )
        value_part = jnp.dot(
            scaled, value_weight[layer_idx].astype(jnp.bfloat16), preferred_element_type=jnp.float32
        )
        gate_sum, value_sum = (
            lax.psum_scatter(gate_part, "cb", scatter_dimension=1, tiled=True),
            lax.psum_scatter(value_part, "cb", scatter_dimension=1, tiled=True),
        )
        share_cols = gate_sum.shape[1]
        first_col = lax.axis_index("cb") * share_cols
        gate_cols = lax.dynamic_slice_in_dim(gate_scale[layer_idx], first_col, share_cols, 0)
        value_cols = lax.dynamic_slice_in_dim(value_scale[layer_idx], first_col, share_cols, 0)
        gate_taps = lax.dynamic_slice_in_dim(conv_gate[layer_idx], first_col, share_cols, 1)
        value_taps = lax.dynamic_slice_in_dim(conv_value[layer_idx], first_col, share_cols, 1)
        gate_pre = inverse * gate_cols * gate_sum
        value_pre = inverse * value_cols * value_sum
        hidden = (
            jax.nn.gelu(causal_taps(gate_pre, gate_taps), approximate=True)
            * causal_taps(value_pre, value_taps)
        ).astype(jnp.bfloat16)
        hidden = lax.all_gather(hidden, "cb", axis=1, tiled=True)
        partial_value = jnp.dot(
            hidden, down_weight[layer_idx].astype(jnp.bfloat16), preferred_element_type=jnp.float32
        )
        down_total = lax.psum(partial_value, "ra")
        current = (residual_weight * state_wide + down_scale[layer_idx] * down_total).astype(
            jnp.bfloat16
        )
    state_wide = current.astype(jnp.float32)
    inverse = row_inverse(state_wide, model_width)
    return (state_wide * inverse * norm_gains[layer_count]).astype(jnp.bfloat16)


def solution(mesh):
    in_specs = (
        P("grp", "cb"),
        P(None, "cb"),
        P(None, "cb", "ra"),
        P(None, "cb", "ra"),
        P(None, "ra"),
        P(None, "ra"),
        P(None, None, "ra"),
        P(None, None, "ra"),
        P(None, "ra", "cb"),
        P(None, "cb"),
    )
    out_specs = P("grp", "cb")
    return jax.shard_map(
        on_device, mesh=mesh, in_specs=in_specs, out_specs=out_specs, check_vma=False
    )
```

profile of v0, /device:TPU:0, one launch (start us, length us, event | category | flops | bytes accessed | tf_op | source)
XLA Modules:
  0.0 362.3 jit_solution(13226815253919093914)
XLA Ops:
  6.5 0.8 fusion.77
  7.4 8.6 %convert.12 = bf16[2,1024,2816]{2,1,0:T(8,128)(2,1)S(1)} convert(f32[2,1024,2816]{2,1,0:T(8,128)} %param.12) | non-fusion elementwise | flops 5767168 | bytes 34603008 | tf_op jit(solution)/shard_map/convert.5
  16.0 4.2 %copy-done.1 = bf16[2,1024,2816]{2,1,0:T(8,128)(2,1)} copy-done((bf16[2,1024,2816]{2,1,0:T(8,128)(2,1)}, bf16[2,1024,2816]{2,1,0:T(8,128)(2,1)S(1)}, u32[]{:S(2)}) %copy-start.1) | copy-done | bytes 11534360
  20.2 4.1 %fusion.5 = f32[256,2816]{0,1:T(8,128)} fusion(bf16[2,1024,2816]{2,1,0:T(8,128)(2,1)S(1)} %convert.12, bf16[256,1024]{1,0:T(8,128)(2,1)S(1)} %copy-done.2, f32[1024]{0:T(1024)S(1)} %bitcast.42), kind=kOutput, calls=%fused_computation.11 | convolution fusion | flops 1477181440 | bytes 9179136 | tf_op jit(solution)/shard_map/dot_general | solution.py:44
  24.3 0.0 reduce-scatter.5.cloned.1.call-update
  24.3 0.0 reduce-scatter.7.cloned.1.call-start
  24.4 8.6 %convert.13 = bf16[2,1024,2816]{2,1,0:T(8,128)(2,1)S(1)} convert(f32[2,1024,2816]{2,1,0:T(8,128)} %param.13) | non-fusion elementwise | flops 5767168 | bytes 34603008 | tf_op jit(solution)/shard_map/convert.4
  32.9 4.8 %copy-done = bf16[2,1024,2816]{2,1,0:T(8,128)(2,1)} copy-done((bf16[2,1024,2816]{2,1,0:T(8,128)(2,1)}, bf16[2,1024,2816]{2,1,0:T(8,128)(2,1)S(1)}, u32[]{:S(2)}) %copy-start) | copy-done | bytes 11534360
  37.8 4.0 %fusion.4 = f32[256,2816]{0,1:T(8,128)} fusion(bf16[2,1024,2816]{2,1,0:T(8,128)(2,1)S(1)} %convert.13, bf16[256,1024]{1,0:T(8,128)(2,1)S(1)} %copy-done.2, f32[1024]{0:T(1024)S(1)} %bitcast.43), kind=kOutput, calls=%fused_computation.9 | convolution fusion | flops 1477181440 | bytes 9179136 | tf_op jit(solution)/shard_map/dot_general | solution.py:47
  41.8 0.0 reduce-scatter.7.cloned.1.call-update
  41.8 0.0 all-gather.3.cloned.1.call-start
  41.9 0.1 fusion.55
  42.0 0.2 fusion.11
  42.2 9.0 %psum.35 = f32[256,1]{0,1:T(1,128)S(1)} all-reduce(f32[256,1]{0,1:T(1,128)S(1)} %bitcast.39), channel_id=1, replica_groups=mesh['grp'=2,'ra'=4,'cb'=4] {'cb'}, use_global_device_ids=true, to_apply=%region_1.0 | all-reduce | flops 256 | bytes 2048 | tf_op jit(solution)/shard_map/psum | solution.py:21
  51.2 0.1 fusion.73
  51.3 0.1 fusion.74
  51.3 0.1 fusion.63
  51.5 12.1 %reduce-scatter.5.cloned.1.call-done = f32[256,704]{0,1:T(8,128)} async-done(((f32[256,2816]{0,1:T(8,128)}), f32[256,704]{0,1:T(8,128)}) %reduce-scatter.5.cloned.1.call-update) | async-done | bytes 720912 | tf_op jit(solution)/shard_map/reduce_scatter | solution.py:51
  63.5 38.8 %reduce-scatter.7.cloned.1.call-done = f32[256,704]{0,1:T(8,128)} async-done(((f32[256,2816]{0,1:T(8,128)}), f32[256,704]{0,1:T(8,128)}) %reduce-scatter.7.cloned.1.call-update) | async-done | bytes 720912 | tf_op jit(solution)/shard_map/reduce_scatter | solution.py:52
  102.3 1.6 multiply_multiply_fusion.4
  103.9 2.2 fusion.25
  106.1 0.0 all-gather.3.cloned.1.call-update
  106.1 0.0 all-reduce.7.cloned.1.call-start
  106.2 12.6 %convert.14 = bf16[2,2816,1024]{2,1,0:T(8,128)(2,1)} convert(f32[2,2816,1024]{2,1,0:T(8,128)} %param.18) | non-fusion elementwise | flops 5767168 | bytes 34603008 | tf_op jit(solution)/shard_map/convert.3
  118.8 6.4 %all-gather.3.cloned.1.call-done = bf16[256,2816]{0,1:T(8,128)(2,1)} async-done(((bf16[256,704]{0,1:T(8,128)(2,1)}), bf16[256,2816]{0,1:T(8,128)(2,1)}) %all-gather.3.cloned.1.call-update) | async-done | bytes 1441808 | tf_op jit(solution)/shard_map/all_gather | solution.py:66
  125.2 5.8 %fusion.3 = f32[256,1024]{1,0:T(8,128)} fusion(bf16[256,2816]{0,1:T(8,128)(2,1)} %all-gather.3.cloned.1.call-done, bf16[2,2816,1024]{2,1,0:T(8,128)(2,1)} %convert.14), kind=kOutput, calls=%fused_computation.7 | convolution fusion | flops 1476395008 | bytes 8257536 | tf_op jit(solution)/shard_map/dot_general | solution.py:67
  130.9 0.0 all-reduce.7.cloned.1.call-update
  130.9 0.0 reduce-scatter.9.cloned.1.call-start
  131.0 52.0 %all-reduce.7.cloned.1.call-done = f32[256,1024]{1,0:T(8,128)} async-done(((f32[256,1024]{1,0:T(8,128)}), f32[256,1024]{1,0:T(8,128)}) %all-reduce.7.cloned.1.call-update) | async-done | bytes 1048592 | tf_op jit(solution)/shard_map/psum | solution.py:70
  183.0 1.5 fusion.15
  184.5 6.6 %fusion.2 = f32[256,2816]{0,1:T(8,128)} fusion(bf16[2,1024,2816]{2,1,0:T(8,128)(2,1)} %copy-done.1, bf16[256,1024]{1,0:T(8,128)(2,1)S(1)} %get-tuple-element.20, f32[1024]{0:T(1024)S(1)} %bitcast.40), kind=kOutput, calls=%fused_computation.5 | convolution fusion | flops 1477181440 | bytes 9179136 | tf_op jit(solution)/shard_map/dot_general | solution.py:44
  191.2 0.2 reduce-scatter.11.cloned.1.call-start
  191.4 6.6 %fusion.1 = f32[256,2816]{0,1:T(8,128)} fusion(bf16[2,1024,2816]{2,1,0:T(8,128)(2,1)} %copy-done, bf16[256,1024]{1,0:T(8,128)(2,1)S(1)} %get-tuple-element.20, f32[1024]{0:T(1024)S(1)} %bitcast.41), kind=kOutput, calls=%fused_computation.3 | convolution fusion | flops 1477181440 | bytes 9179136 | tf_op jit(solution)/shard_map/dot_general | solution.py:47
  198.1 0.0 all-gather.5.cloned.1.call-start
  198.1 0.1 fusion.59
  198.2 0.1 fusion.69
  198.3 6.8 %psum.37 = f32[256,1]{0,1:T(1,128)S(1)} all-reduce(f32[256,1]{0,1:T(1,128)S(1)} %bitcast.34), channel_id=1, replica_groups=mesh['grp'=2,'ra'=4,'cb'=4] {'cb'}, use_global_device_ids=true, to_apply=%region_6.7 | all-reduce | flops 256 | bytes 2048 | tf_op jit(solution)/shard_map/psum | solution.py:21
  205.2 21.6 %reduce-scatter.9.cloned.1.call-done = f32[256,704]{0,1:T(8,128)} async-done(((f32[256,2816]{0,1:T(8,128)}), f32[256,704]{0,1:T(8,128)}) %reduce-scatter.9.cloned.1.call-update) | async-done | bytes 720912 | tf_op jit(solution)/shard_map/reduce_scatter | solution.py:51
  226.8 38.6 %reduce-scatter.11.cloned.1.call-done = f32[256,704]{0,1:T(8,128)} async-done(((f32[256,2816]{0,1:T(8,128)}), f32[256,704]{0,1:T(8,128)}) %reduce-scatter.11.cloned.1.call-update) | async-done | bytes 720912 | tf_op jit(solution)/shard_map/reduce_scatter | solution.py:52
  265.4 1.6 multiply_multiply_fusion.2
  267.0 2.2 fusion.34
  269.2 0.0 all-reduce.9.cloned.1.call-start
  269.3 19.0 %all-gather.5.cloned.1.call-done = bf16[256,2816]{0,1:T(8,128)(2,1)} async-done(((bf16[256,704]{0,1:T(8,128)(2,1)}), bf16[256,2816]{0,1:T(8,128)(2,1)}) %all-gather.5.cloned.1.call-update) | async-done | bytes 1441808 | tf_op jit(solution)/shard_map/all_gather | solution.py:66
  288.3 5.7 %fusion = f32[256,1024]{1,0:T(8,128)} fusion(bf16[256,2816]{0,1:T(8,128)(2,1)} %all-gather.5.cloned.1.call-done, bf16[2,2816,1024]{2,1,0:T(8,128)(2,1)} %convert.14), kind=kOutput, calls=%fused_computation.1 | convolution fusion | flops 1476395008 | bytes 8257536 | tf_op jit(solution)/shard_map/dot_general | solution.py:67
  294.0 52.1 %all-reduce.9.cloned.1.call-done = f32[256,1024]{1,0:T(8,128)} async-done(((f32[256,1024]{1,0:T(8,128)}), f32[256,1024]{1,0:T(8,128)}) %all-reduce.9.cloned.1.call-update) | async-done | bytes 1048592 | tf_op jit(solution)/shard_map/psum | solution.py:70
  346.1 1.5 fusion.6
  347.6 6.8 %psum.39 = f32[256,1]{0,1:T(1,128)S(1)} all-reduce(f32[256,1]{0,1:T(1,128)S(1)} %bitcast.37), channel_id=1, replica_groups=mesh['grp'=2,'ra'=4,'cb'=4] {'cb'}, use_global_device_ids=true, to_apply=%region_11.12 | all-reduce | flops 256 | bytes 2048 | tf_op jit(solution)/shard_map/psum | solution.py:21
  354.5 1.0 fusion.8
  (25 shorter events, 0.2 us)
Async XLA Ops:
  6.5 57.0 %reduce-scatter.5.cloned.1.call-start = ((), (), s32[]{:S(2)}) async-start(), calls=%async_computation.4 | async-start | bytes 3604480 | tf_op jit(solution)/shard_map/reduce_scatter | solution.py:51
  7.4 12.8 %copy-start.2 = (bf16[256,1024]{1,0:T(8,128)(2,1)S(1)}, bf16[256,1024]{1,0:T(8,128)(2,1)}, u32[]{:S(2)}) copy-start(bf16[256,1024]{1,0:T(8,128)(2,1)} %param.10) | copy-start | bytes 1572868
  16.0 4.2 %copy-start.1 = (bf16[2,1024,2816]{2,1,0:T(8,128)(2,1)}, bf16[2,1024,2816]{2,1,0:T(8,128)(2,1)S(1)}, u32[]{:S(2)}) copy-start(bf16[2,1024,2816]{2,1,0:T(8,128)(2,1)S(1)} %convert.12) | copy-start | bytes 34603012
  24.3 78.0 %reduce-scatter.7.cloned.1.call-start = ((), (), s32[]{:S(2)}) async-start(), calls=%async_computation.5 | async-start | bytes 3604480 | tf_op jit(solution)/shard_map/reduce_scatter | solution.py:52
  32.9 4.8 %copy-start = (bf16[2,1024,2816]{2,1,0:T(8,128)(2,1)}, bf16[2,1024,2816]{2,1,0:T(8,128)(2,1)S(1)}, u32[]{:S(2)}) copy-start(bf16[2,1024,2816]{2,1,0:T(8,128)(2,1)S(1)} %convert.13) | copy-start | bytes 34603012
  37.7 4.1 %copy-start.5 = (f32[2,2816]{1,0:T(2,128)S(1)}, f32[2,2816]{1,0:T(2,128)}, u32[]{:S(2)}) copy-start(f32[2,2816]{1,0:T(2,128)} %param.14) | copy-start | bytes 67588
  37.7 4.1 %copy-start.6 = (f32[2,2816]{1,0:T(2,128)S(1)}, f32[2,2816]{1,0:T(2,128)}, u32[]{:S(2)}) copy-start(f32[2,2816]{1,0:T(2,128)} %param.15) | copy-start | bytes 67588
  37.8 13.5 %copy-start.3 = (f32[2,3,2816]{2,0,1:T(2,128)S(1)}, f32[2,3,2816]{2,0,1:T(2,128)}, u32[]{:S(2)}) copy-start(f32[2,3,2816]{2,0,1:T(2,128)} %param.16) | copy-start | bytes 202756
  37.8 13.5 %copy-start.4 = (f32[2,3,2816]{2,0,1:T(2,128)S(1)}, f32[2,3,2816]{2,0,1:T(2,128)}, u32[]{:S(2)}) copy-start(f32[2,3,2816]{2,0,1:T(2,128)} %param.17) | copy-start | bytes 202756
  41.8 83.4 %all-gather.3.cloned.1.call-start = ((), (), s32[]{:S(2)}) async-start(), calls=%async_computation.6 | async-start | bytes 1802240 | tf_op jit(solution)/shard_map/all_gather | solution.py:66
  106.1 76.9 %all-reduce.7.cloned.1.call-start = ((), (), s32[]{:S(2)}) async-start(), calls=%async_computation.7 | async-start | bytes 2097152 | tf_op jit(solution)/shard_map/psum | solution.py:70
  118.8 12.2 %copy-start.7 = (f32[2,1024]{1,0:T(2,128)S(1)}, f32[2,1024]{1,0:T(2,128)}, u32[]{:S(2)}) copy-start(f32[2,1024]{1,0:T(2,128)} %param.19) | copy-start | bytes 24580
  130.9 95.8 %reduce-scatter.9.cloned.1.call-start = ((), (), s32[]{:S(2)}) async-start(), calls=%async_computation.8 | async-start | bytes 3604480 | tf_op jit(solution)/shard_map/reduce_scatter | solution.py:51
  191.2 74.2 %reduce-scatter.11.cloned.1.call-start = ((), (), s32[]{:S(2)}) async-start(), calls=%async_computation.9 | async-start | bytes 3604480 | tf_op jit(solution)/shard_map/reduce_scatter | solution.py:52
  198.1 90.2 %all-gather.5.cloned.1.call-start = ((), (), s32[]{:S(2)}) async-start(), calls=%async_computation.10 | async-start | bytes 1802240 | tf_op jit(solution)/shard_map/all_gather | solution.py:66
  269.2 76.9 %all-reduce.9.cloned.1.call-start = ((), (), s32[]{:S(2)}) async-start(), calls=%async_computation.11 | async-start | bytes 2097152 | tf_op jit(solution)/shard_map/psum | solution.py:70
Sparse Core Ops, SparseCore 0:
  24.4 39.0 reduce-scatter.4
  66.1 36.1 reduce-scatter.6
  106.2 18.8 all-gather.2
  131.1 51.8 all-reduce.6
  191.3 35.4 reduce-scatter.8
  229.2 36.1 reduce-scatter.10
  269.3 18.8 all-gather.4
  294.1 51.8 all-reduce.8
where the time goes:
time: 363 us; the launch traced here: 362 us
  waiting for transfers between devices  241 us (66%)
  other arithmetic  41.6 us (11%)
  matrix products  32.8 us (9%)
  blocking collectives  22.7 us (6%)
  between operations  13.7 us (4%)
  local copies, waits for them, and re-layouts  10.5 us (3%)
    psum x2, waiting for transfers between devices, on_device(): down_total = lax.psum(partial_value, 'ra')  104 us
    reduce_scatter x2, waiting for transfers between devices, on_device(): lax.psum_scatter(value_part, 'cb', scatter_dimension=1, tiled=True)  77.4 us
    reduce_scatter x2, waiting for transfers between devices, on_device(): lax.psum_scatter(gate_part, 'cb', scatter_dimension=1, tiled=True)  33.6 us
    another operation x3, other arithmetic  29.8 us
    all_gather x2, waiting for transfers between devices, on_device(): hidden = lax.all_gather(hidden, 'cb', axis=1, tiled=True)  25.4 us
    psum x3, blocking collectives, row_inverse(): lax.psum(jnp.sum(state_wide * state_wide, axis=1, keepdims=True), 'cb')  22.7 us
    dot_general x2, matrix products, on_device(): jnp.dot(hidden, down_weight[layer_idx].astype(jnp.bfloat16), preferred_el...  11.5 us
    dot_general x2, matrix products, on_device(): jnp.dot(scaled, gate_weight[layer_idx].astype(jnp.bfloat16), preferred_el...  10.7 us
  transfers between devices with their start and end apart: 8, of which 8 were waited for; matrix products, arithmetic and copies ran while one was open for 9% of the time, Pallas kernels for 0%

commit v1 on v0

--- a/solution.py
+++ b/solution.py
@@ -67,7 +67,7 @@
         partial_value = jnp.dot(
             hidden, down_weight[layer_idx].astype(jnp.bfloat16), preferred_element_type=jnp.float32
         )
-        down_total = lax.psum(partial_value, "ra")
+        down_total = jnp.sum(lax.all_gather(partial_value, "ra"), axis=0)
         current = (residual_weight * state_wide + down_scale[layer_idx] * down_total).astype(
             jnp.bfloat16
         )

time: 363 us -> 422 us (1.16)
  waiting for transfers between devices: 241 us -> 298 us
    all_gather x0 -> x2, waiting for transfers between devices: none -> 162 us  [on_device(): down_total = jnp.sum(lax.all_gather(partial_value, 'ra'), axis=0)]
    psum x2 -> x0, waiting for transfers between devices: 104 us -> none  [on_device(): down_total = lax.psum(partial_value, 'ra')]
    reduce_sum x0 -> x2, other arithmetic: none -> 5.44 us  [on_device(): down_total = jnp.sum(lax.all_gather(partial_value, 'ra'), axis=0)]
  transfers between devices with their start and end apart: 8 -> 8, of which waited for: 8 -> 8; matrix products, arithmetic and copies ran while one was open for 9% -> 8% of each run, Pallas kernels for 0% -> 0%
where the time goes in v1:
time: 422 us
  waiting for transfers between devices  298 us (71%)
  other arithmetic  44.6 us (11%)
  matrix products  32.8 us (8%)
  blocking collectives  21.9 us (5%)
  between operations  13.7 us (3%)
  local copies, waits for them, and re-layouts  10.5 us (2%)
    all_gather x2, waiting for transfers between devices, on_device(): down_total = jnp.sum(lax.all_gather(partial_value, 'ra'), axis=0)  162 us
    reduce_scatter x2, waiting for transfers between devices, on_device(): lax.psum_scatter(value_part, 'cb', scatter_dimension=1, tiled=True)  77.4 us
    reduce_scatter x2, waiting for transfers between devices, on_device(): lax.psum_scatter(gate_part, 'cb', scatter_dimension=1, tiled=True)  33.5 us
    another operation x3, other arithmetic  29.8 us
    all_gather x2, waiting for transfers between devices, on_device(): hidden = lax.all_gather(hidden, 'cb', axis=1, tiled=True)  25.4 us
    psum x3, blocking collectives, row_inverse(): lax.psum(jnp.sum(state_wide * state_wide, axis=1, keepdims=True), 'cb')  21.9 us
    dot_general x2, matrix products, on_device(): jnp.dot(hidden, down_weight[layer_idx].astype(jnp.bfloat16), preferred_el...  11.5 us
    dot_general x2, matrix products, on_device(): jnp.dot(scaled, gate_weight[layer_idx].astype(jnp.bfloat16), preferred_el...  10.7 us
  transfers between devices with their start and end apart: 8, of which 8 were waited for; matrix products, arithmetic and copies ran while one was open for 8% of the time, Pallas kernels for 0%

profile of v1, /device:TPU:0, one launch (start us, length us, event | category | flops | bytes accessed | tf_op | source)
XLA Modules:
  0.0 421.8 jit_solution(424893775356549077)
XLA Ops:
  6.5 0.8 fusion.77
  7.4 8.6 %convert.12 = bf16[2,1024,2816]{2,1,0:T(8,128)(2,1)S(1)} convert(f32[2,1024,2816]{2,1,0:T(8,128)} %param.12) | non-fusion elementwise | flops 5767168 | bytes 34603008 | tf_op jit(solution)/shard_map/convert.5
  16.0 4.2 copy-done.1
  20.2 4.1 fusion.5
  24.3 0.0 reduce-scatter.5.cloned.1.call-update
  24.3 0.0 reduce-scatter.7.cloned.1.call-start
  24.4 8.6 %convert.13 = bf16[2,1024,2816]{2,1,0:T(8,128)(2,1)S(1)} convert(f32[2,1024,2816]{2,1,0:T(8,128)} %param.13) | non-fusion elementwise | flops 5767168 | bytes 34603008 | tf_op jit(solution)/shard_map/convert.4
  32.9 4.8 %copy-done = bf16[2,1024,2816]{2,1,0:T(8,128)(2,1)} copy-done((bf16[2,1024,2816]{2,1,0:T(8,128)(2,1)}, bf16[2,1024,2816]{2,1,0:T(8,128)(2,1)S(1)}, u32[]{:S(2)}) %copy-start) | copy-done | bytes 11534360
  37.8 4.0 fusion.4
  41.8 0.0 reduce-scatter.7.cloned.1.call-update
  41.8 0.0 all-gather.7.cloned.1.call-start
  41.9 0.1 fusion.55
  42.0 0.2 fusion.11
  42.2 9.0 %psum.21 = f32[256,1]{0,1:T(1,128)S(1)} all-reduce(f32[256,1]{0,1:T(1,128)S(1)} %bitcast.43), channel_id=1, replica_groups=mesh['grp'=2,'ra'=4,'cb'=4] {'cb'}, use_global_device_ids=true, to_apply=%region_1.0 | all-reduce | flops 256 | bytes 2048 | tf_op jit(solution)/shard_map/psum | solution.py:21
  51.2 0.1 fusion.73
  51.3 0.1 fusion.74
  51.3 0.1 fusion.63
  51.5 12.1 %reduce-scatter.5.cloned.1.call-done = f32[256,704]{0,1:T(8,128)} async-done(((f32[256,2816]{0,1:T(8,128)}), f32[256,704]{0,1:T(8,128)}) %reduce-scatter.5.cloned.1.call-update) | async-done | bytes 720912 | tf_op jit(solution)/shard_map/reduce_scatter | solution.py:51
  63.5 38.8 %reduce-scatter.7.cloned.1.call-done = f32[256,704]{0,1:T(8,128)} async-done(((f32[256,2816]{0,1:T(8,128)}), f32[256,704]{0,1:T(8,128)}) %reduce-scatter.7.cloned.1.call-update) | async-done | bytes 720912 | tf_op jit(solution)/shard_map/reduce_scatter | solution.py:52
  102.3 1.6 multiply_multiply_fusion.4
  103.9 2.2 fusion.25
  106.1 0.0 all-gather.11.cloned.1.call-start
  106.2 12.6 %convert.14 = bf16[2,2816,1024]{2,1,0:T(8,128)(2,1)} convert(f32[2,2816,1024]{2,1,0:T(8,128)} %param.18) | non-fusion elementwise | flops 5767168 | bytes 34603008 | tf_op jit(solution)/shard_map/convert.3
  118.8 6.4 %all-gather.7.cloned.1.call-done = bf16[256,2816]{0,1:T(8,128)(2,1)} async-done(((bf16[256,704]{0,1:T(8,128)(2,1)}), bf16[256,2816]{0,1:T(8,128)(2,1)}) %all-gather.7.cloned.1.call-update) | async-done | bytes 1441808 | tf_op jit(solution)/shard_map/all_gather | solution.py:66
  125.2 5.7 %fusion.3 = f32[256,1024]{1,0:T(8,128)} fusion(bf16[256,2816]{0,1:T(8,128)(2,1)} %all-gather.7.cloned.1.call-done, bf16[2,2816,1024]{2,1,0:T(8,128)(2,1)} %convert.14), kind=kOutput, calls=%fused_computation.7 | convolution fusion | flops 1476395008 | bytes 8257536 | tf_op jit(solution)/shard_map/dot_general | solution.py:67
  130.9 0.2 reduce-scatter.9.cloned.1.call-start
  131.2 80.6 %all-gather.11.cloned.1.call-done = f32[1024,1024]{1,0:T(8,128)} async-done(((f32[256,1024]{1,0:T(8,128)}), f32[1024,1024]{1,0:T(8,128)}) %all-gather.11.cloned.1.call-update) | async-done | bytes 4194320 | tf_op jit(solution)/shard_map/all_gather | solution.py:70
  211.8 2.7 reduce_sum.46
  214.5 0.3 fusion.15
  214.8 6.6 %fusion.2 = f32[256,2816]{0,1:T(8,128)} fusion(bf16[2,1024,2816]{2,1,0:T(8,128)(2,1)} %copy-done.1, bf16[256,1024]{1,0:T(8,128)(2,1)S(1)} %get-tuple-element.20, f32[1024]{0:T(1024)S(1)} %bitcast.44), kind=kOutput, calls=%fused_computation.5 | convolution fusion | flops 1477181440 | bytes 9179136 | tf_op jit(solution)/shard_map/dot_general | solution.py:44
  221.5 0.0 reduce-scatter.11.cloned.1.call-start
  221.5 6.6 %fusion.1 = f32[256,2816]{0,1:T(8,128)} fusion(bf16[2,1024,2816]{2,1,0:T(8,128)(2,1)} %copy-done, bf16[256,1024]{1,0:T(8,128)(2,1)S(1)} %get-tuple-element.20, f32[1024]{0:T(1024)S(1)} %bitcast.45), kind=kOutput, calls=%fused_computation.3 | convolution fusion | flops 1477181440 | bytes 9179136 | tf_op jit(solution)/shard_map/dot_general | solution.py:47
  228.2 0.0 all-gather.9.cloned.1.call-start
  228.2 0.1 fusion.59
  228.3 0.1 fusion.69
  228.5 6.4 %psum.22 = f32[256,1]{0,1:T(1,128)S(1)} all-reduce(f32[256,1]{0,1:T(1,128)S(1)} %bitcast.38), channel_id=1, replica_groups=mesh['grp'=2,'ra'=4,'cb'=4] {'cb'}, use_global_device_ids=true, to_apply=%region_6.7 | all-reduce | flops 256 | bytes 2048 | tf_op jit(solution)/shard_map/psum | solution.py:21
  234.9 21.4 %reduce-scatter.9.cloned.1.call-done = f32[256,704]{0,1:T(8,128)} async-done(((f32[256,2816]{0,1:T(8,128)}), f32[256,704]{0,1:T(8,128)}) %reduce-scatter.9.cloned.1.call-update) | async-done | bytes 720912 | tf_op jit(solution)/shard_map/reduce_scatter | solution.py:51
  256.3 38.6 %reduce-scatter.11.cloned.1.call-done = f32[256,704]{0,1:T(8,128)} async-done(((f32[256,2816]{0,1:T(8,128)}), f32[256,704]{0,1:T(8,128)}) %reduce-scatter.11.cloned.1.call-update) | async-done | bytes 720912 | tf_op jit(solution)/shard_map/reduce_scatter | solution.py:52
  294.9 1.6 multiply_multiply_fusion.2
  296.5 2.2 fusion.34
  298.8 0.0 all-gather.13.cloned.1.call-start
  298.8 19.0 %all-gather.9.cloned.1.call-done = bf16[256,2816]{0,1:T(8,128)(2,1)} async-done(((bf16[256,704]{0,1:T(8,128)(2,1)}), bf16[256,2816]{0,1:T(8,128)(2,1)}) %all-gather.9.cloned.1.call-update) | async-done | bytes 1441808 | tf_op jit(solution)/shard_map/all_gather | solution.py:66
  317.8 5.7 %fusion = f32[256,1024]{1,0:T(8,128)} fusion(bf16[256,2816]{0,1:T(8,128)(2,1)} %all-gather.9.cloned.1.call-done, bf16[2,2816,1024]{2,1,0:T(8,128)(2,1)} %convert.14), kind=kOutput, calls=%fused_computation.1 | convolution fusion | flops 1476395008 | bytes 8257536 | tf_op jit(solution)/shard_map/dot_general | solution.py:67
  323.6 80.9 %all-gather.13.cloned.1.call-done = f32[1024,1024]{1,0:T(8,128)} async-done(((f32[256,1024]{1,0:T(8,128)}), f32[1024,1024]{1,0:T(8,128)}) %all-gather.13.cloned.1.call-update) | async-done | bytes 4194320 | tf_op jit(solution)/shard_map/all_gather | solution.py:70
  404.5 2.7 reduce_sum.48
  407.2 0.3 fusion.6
  407.5 6.4 %psum.23 = f32[256,1]{0,1:T(1,128)S(1)} all-reduce(f32[256,1]{0,1:T(1,128)S(1)} %bitcast.41), channel_id=1, replica_groups=mesh['grp'=2,'ra'=4,'cb'=4] {'cb'}, use_global_device_ids=true, to_apply=%region_11.12 | all-reduce | flops 256 | bytes 2048 | tf_op jit(solution)/shard_map/psum | solution.py:21
  413.9 1.0 fusion.8
  (27 shorter events, 0.2 us)
Async XLA Ops:
  6.5 57.0 %reduce-scatter.5.cloned.1.call-start = ((), (), s32[]{:S(2)}) async-start(), calls=%async_computation.4 | async-start | bytes 3604480 | tf_op jit(solution)/shard_map/reduce_scatter | solution.py:51
  7.4 12.8 %copy-start.2 = (bf16[256,1024]{1,0:T(8,128)(2,1)S(1)}, bf16[256,1024]{1,0:T(8,128)(2,1)}, u32[]{:S(2)}) copy-start(bf16[256,1024]{1,0:T(8,128)(2,1)} %param.10) | copy-start | bytes 1572868
  16.0 4.2 copy-start.1
  24.3 78.0 %reduce-scatter.7.cloned.1.call-start = ((), (), s32[]{:S(2)}) async-start(), calls=%async_computation.5 | async-start | bytes 3604480 | tf_op jit(solution)/shard_map/reduce_scatter | solution.py:52
  32.9 4.8 %copy-start = (bf16[2,1024,2816]{2,1,0:T(8,128)(2,1)}, bf16[2,1024,2816]{2,1,0:T(8,128)(2,1)S(1)}, u32[]{:S(2)}) copy-start(bf16[2,1024,2816]{2,1,0:T(8,128)(2,1)S(1)} %convert.13) | copy-start | bytes 34603012
  37.7 4.1 copy-start.5
  37.7 4.1 copy-start.6
  37.8 13.5 %copy-start.3 = (f32[2,3,2816]{2,0,1:T(2,128)S(1)}, f32[2,3,2816]{2,0,1:T(2,128)}, u32[]{:S(2)}) copy-start(f32[2,3,2816]{2,0,1:T(2,128)} %param.16) | copy-start | bytes 202756
  37.8 13.5 %copy-start.4 = (f32[2,3,2816]{2,0,1:T(2,128)S(1)}, f32[2,3,2816]{2,0,1:T(2,128)}, u32[]{:S(2)}) copy-start(f32[2,3,2816]{2,0,1:T(2,128)} %param.17) | copy-start | bytes 202756
  41.8 83.4 %all-gather.7.cloned.1.call-start = ((), (), s32[]{:S(2)}) async-start(), calls=%async_computation.6 | async-start | bytes 1802240 | tf_op jit(solution)/shard_map/all_gather | solution.py:66
  106.1 105.7 %all-gather.11.cloned.1.call-start = ((), (), s32[]{:S(2)}) async-start(), calls=%async_computation.10 | async-start | bytes 5242880 | tf_op jit(solution)/shard_map/all_gather | solution.py:70
  118.8 12.3 %copy-start.7 = (f32[2,1024]{1,0:T(2,128)S(1)}, f32[2,1024]{1,0:T(2,128)}, u32[]{:S(2)}) copy-start(f32[2,1024]{1,0:T(2,128)} %param.19) | copy-start | bytes 24580
  130.9 125.4 %reduce-scatter.9.cloned.1.call-start = ((), (), s32[]{:S(2)}) async-start(), calls=%async_computation.7 | async-start | bytes 3604480 | tf_op jit(solution)/shard_map/reduce_scatter | solution.py:51
  221.5 73.5 %reduce-scatter.11.cloned.1.call-start = ((), (), s32[]{:S(2)}) async-start(), calls=%async_computation.8 | async-start | bytes 3604480 | tf_op jit(solution)/shard_map/reduce_scatter | solution.py:52
  228.2 89.6 %all-gather.9.cloned.1.call-start = ((), (), s32[]{:S(2)}) async-start(), calls=%async_computation.9 | async-start | bytes 1802240 | tf_op jit(solution)/shard_map/all_gather | solution.py:66
  298.8 105.7 %all-gather.13.cloned.1.call-start = ((), (), s32[]{:S(2)}) async-start(), calls=%async_computation.11 | async-start | bytes 5242880 | tf_op jit(solution)/shard_map/all_gather | solution.py:70
Sparse Core Ops, SparseCore 0:
  24.4 39.0 reduce-scatter.4
  66.1 36.1 reduce-scatter.6
  106.2 18.8 all-gather.6
  131.0 80.7 all-gather.10
  221.6 34.6 reduce-scatter.8
  258.7 36.1 reduce-scatter.10
  298.9 18.8 all-gather.8
  323.7 80.7 all-gather.12
